TPU v7x, 32 devices: a whole 2x2x4 slice. The times are simulated.
32 devices in a mesh: grp: 2 (over y), kv: 4 (over z), tp: 4 (over x, core).
Axes of the slice: x: 2, y: 2, z: 4, core: 2. Of those that a mesh axis runs over, the one named last changes fastest.
Arguments:
- tokens: bfloat16 [16, 4096], P('grp', 'kv'), parts along dimension 0, may hold values from -6 to 6
- norm_gain: float32 [4096], replicated, may hold values from 0.1 to 1.9
- w_query: bfloat16 [4096, 4096], P('kv', 'tp'), may hold values from -0.09375 to 0.09375
- key_weight: bfloat16 [4096, 512], P('kv', 'tp'), may hold values from -0.09375 to 0.09375
- value_weight: bfloat16 [4096, 512], P('kv', 'tp'), may hold values from -0.09375 to 0.09375
- w_gate: bfloat16 [4096, 64], replicated, may hold values from -0.09375 to 0.09375
- gate_bias: float32 [64], replicated, may hold values from -3 to 4
- w_out: bfloat16 [4096, 4096], P('kv', 'tp'), may hold values from -0.1875 to 0.1875
- cache_keys: bfloat16 [16, 3072, 512], P('grp', 'kv', 'tp'), parts along dimension 0, may hold values from -240 to 240
- cache_values: bfloat16 [16, 3072, 512], P('grp', 'kv', 'tp'), parts along dimension 0, may hold values from -8 to 8
- cache_gate: float32 [16, 64, 3072], P('grp', 'tp', 'kv'), parts along dimension 0, may hold values from -3072 to 0, as said below
- gate_total: float32 [16, 64], P('grp', 'tp'), parts along dimension 0, may hold values from -3072 to 0, as said below
- lengths: int32 [16], P('grp'), parts along dimension 0, may hold values from 1536 to 3072, as said below
Outputs:
- mixed: bfloat16 [16, 4096], P('grp', 'kv'), parts along dimension 0
- key_new: bfloat16 [16, 512], P('grp', 'tp'), parts along dimension 0
- value_new: bfloat16 [16, 512], P('grp', 'tp'), parts along dimension 0
There are 2 independent parts, one for each index of `grp`. A program takes and returns all parts, laid end to end along the dimension named above; an argument that names none is the same for every part. Nothing has to cross between parts.
Inputs may be any that keep to these rules, and one draw needn't show every extreme that they name: `lengths`: one sequence of each draw has all 3072 positions cached. `cache_gate`: non-increasing along positions. `gate_total`: equal to cache_gate at position lengths - 1 of the same sequence and head.
All inputs are finite; a program needn't handle non-finite values.
Results may differ from a plain program's by a relative error of at most 0.015.
Values may be sent and summed in bfloat16 or wider, within the bound.
A program may use at most 64 MiB of HBM per device.

v0:
```python
import jax
import jax.numpy as jnp
from jax import lax
from jax.sharding import PartitionSpec as P

HEAD_SIZE = 64
NEG_FILL = -1e30


def per_device(
    tokens,
    norm_gain,
    w_query,
    key_weight,
    value_weight,
    w_gate,
    gate_bias,
    w_out,
    cache_keys,
    cache_values,
    cache_gate,
    gate_total,
    lengths,
):
    seq_count = tokens.shape[0]
    width_dev = tokens.shape[1]
    heads_dev = cache_gate.shape[1]
    positions_dev = cache_gate.shape[2]
    kv_heads_dev = cache_keys.shape[2] // HEAD_SIZE
    head_group = heads_dev // kv_heads_dev
    logit_scale = HEAD_SIZE ** (-0.5)
    whole = lax.all_gather(tokens, "kv", axis=1, tiled=True)
    features = whole.astype(jnp.float32)
    normed = (
        features
        * lax.rsqrt(jnp.mean(features * features, axis=-1, keepdims=True) + 1e-06)
        * norm_gain
    )
    normed = normed.astype(jnp.bfloat16)
    kv_index = lax.axis_index("kv")
    tp_index = lax.axis_index("tp")
    own_rows = lax.dynamic_slice_in_dim(normed, kv_index * width_dev, width_dev, 1)
    query_part = jnp.dot(own_rows, w_query, preferred_element_type=jnp.float32)
    key_part = jnp.dot(own_rows, key_weight, preferred_element_type=jnp.float32)
    value_part = jnp.dot(own_rows, value_weight, preferred_element_type=jnp.float32)
    query_sum, key_sum, value_sum = lax.psum((query_part, key_part, value_part), "kv")
    query = query_sum.astype(jnp.bfloat16)
    key_new = key_sum.astype(jnp.bfloat16)
    value_new = value_sum.astype(jnp.bfloat16)
    gate_cols = lax.dynamic_slice_in_dim(w_gate, tp_index * heads_dev, heads_dev, 1)
    bias_cols = lax.dynamic_slice_in_dim(gate_bias, tp_index * heads_dev, heads_dev, 0)
    log_gate = jax.nn.log_sigmoid(
        jnp.dot(normed, gate_cols, preferred_element_type=jnp.float32) + bias_cols
    )
    level = gate_total + log_gate
    query_head_rows = query.reshape(seq_count, kv_heads_dev, head_group, HEAD_SIZE)
    key_block = cache_keys.reshape(seq_count, positions_dev, kv_heads_dev, HEAD_SIZE)
    value_block = cache_values.reshape(seq_count, positions_dev, kv_heads_dev, HEAD_SIZE)
    score_matrix = (
        jnp.einsum(
            "skgd,spkd->skgp", query_head_rows, key_block, preferred_element_type=jnp.float32
        )
        * logit_scale
    )
    forget_bias = (level[:, :, None] - cache_gate).reshape(
        seq_count, kv_heads_dev, head_group, positions_dev
    )
    positions = kv_index * positions_dev + jnp.arange(positions_dev, dtype=jnp.int32)
    valid_mask = (positions[None, :] < lengths[:, None])[:, None, None, :]
    score_matrix = jnp.where(valid_mask, score_matrix + forget_bias, NEG_FILL)
    local_max = jnp.max(score_matrix, axis=-1)
    weights = jnp.where(valid_mask, jnp.exp(score_matrix - local_max[..., None]), 0.0)
    local_total = jnp.sum(weights, axis=-1)
    local_values = jnp.einsum(
        "skgp,spkd->skgd",
        weights.astype(jnp.bfloat16),
        value_block,
        preferred_element_type=jnp.float32,
    )
    block_max = lax.pmax(local_max, "kv")
    rescale = jnp.exp(local_max - block_max)
    block_total, block_values = lax.psum(
        (local_total * rescale, local_values * rescale[..., None]), "kv"
    )
    key_current = key_new.reshape(seq_count, kv_heads_dev, HEAD_SIZE)
    current_score = (
        jnp.einsum(
            "skgd,skd->skg", query_head_rows, key_current, preferred_element_type=jnp.float32
        )
        * logit_scale
    )
    top = jnp.maximum(block_max, current_score)
    cached_scale = jnp.exp(block_max - top)
    current_weight = jnp.exp(current_score - top)
    denominator = block_total * cached_scale + current_weight
    value_current = value_new.reshape(seq_count, kv_heads_dev, 1, HEAD_SIZE).astype(jnp.float32)
    total_sum = block_values * cached_scale[..., None] + current_weight[..., None] * value_current
    attended = (
        (total_sum / denominator[..., None])
        .reshape(seq_count, heads_dev * HEAD_SIZE)
        .astype(jnp.bfloat16)
    )
    partial_value = lax.dot_general(
        attended, w_out, (((1,), (1,)), ((), ())), preferred_element_type=jnp.float32
    )
    partial_value = lax.optimization_barrier(partial_value.astype(jnp.bfloat16)).astype(jnp.float32)
    mixed = lax.psum(partial_value.astype(jnp.bfloat16), "tp")
    return (mixed, key_new, value_new)


def solution(mesh):
    placed = (
        P("grp", "kv"),
        P(),
        P("kv", "tp"),
        P("kv", "tp"),
        P("kv", "tp"),
        P(),
        P(),
        P("kv", "tp"),
        P("grp", "kv", "tp"),
        P("grp", "kv", "tp"),
        P("grp", "tp", "kv"),
        P("grp", "tp"),
        P("grp"),
    )
    return jax.shard_map(
        per_device,
        mesh=mesh,
        in_specs=placed,
        out_specs=(P("grp", "kv"), P("grp", "tp"), P("grp", "tp")),
        check_vma=False,
    )
```

profile of v0, /device:TPU:0, one launch (start us, length us, event | category | flops | bytes accessed | tf_op | source)
XLA Modules:
  0.0 91.3 jit_solution(11908319094124294041)
XLA Ops:
  0.7 0.9 dynamic_slice.11
  1.5 0.7 broadcast_compare_fusion
  2.3 15.1 %all_gather.3 = bf16[8,4096]{1,0:T(8,128)(2,1)S(1)} all-gather(bf16[8,1024]{1,0:T(8,128)(2,1)} %param.13), channel_id=1, replica_groups=mesh['grp'=2,'kv'=4,'tp'=4] {'kv'}, dimensions={1}, use_global_device_ids=true | all-gather | bytes 81920 | tf_op jit(solution)/shard_map/all_gather | solution.py:32
  17.4 0.1 fusion.9
  17.5 0.8 fusion.11
  18.4 1.1 %fusion.22 = f32[8,16]{1,0:T(8,128)S(1)} fusion(f32[8,16]{1,0:T(8,128)} %param.24, bf16[8,4096]{1,0:T(8,128)(2,1)S(1)} %fusion.11, bf16[4096,64]{0,1:T(8,128)(2,1)} %param.18, s32[]{:T(128)S(6)} %select_n.20, f32[16]{0:T(128)S(1)} %dynamic_slice.11), kind=kOutput, calls=%fused_computation.35 | convolution fusion | flops 1049856 | bytes 201284 | tf_op jit(solution)/shard_map/dot_general | solution.py:53
  19.4 1.1 %fusion.15 = f32[8,128]{1,0:T(8,128)S(1)} fusion(bf16[1024,128]{1,0:T(8,128)(2,1)} %param.16, bf16[8,4096]{1,0:T(8,128)(2,1)S(1)} %fusion.11, s32[]{:T(128)S(6)} %select_n.19), kind=kOutput, calls=%fused_computation.24 | convolution fusion | flops 2097152 | bytes 282628 | tf_op jit(solution)/shard_map/dot_general | solution.py:44
  20.6 1.1 %fusion.13 = f32[8,128]{1,0:T(8,128)S(1)} fusion(bf16[1024,128]{1,0:T(8,128)(2,1)} %param.17, bf16[8,4096]{1,0:T(8,128)(2,1)S(1)} %fusion.11, s32[]{:T(128)S(6)} %select_n.19), kind=kOutput, calls=%fused_computation.22 | convolution fusion | flops 2097152 | bytes 282628 | tf_op jit(solution)/shard_map/dot_general | solution.py:45
  21.7 0.4 fusion.17
  22.0 19.1 %psum.42 = bf16[8,1024]{1,0:T(8,128)(2,1)S(1)} all-reduce(f32[8,1024]{1,0:T(8,128)S(1)} %fusion.17), channel_id=1, replica_groups=mesh['grp'=2,'kv'=4,'tp'=4] {'kv'}, use_global_device_ids=true, to_apply=%region_1.0 | all-reduce | flops 8192 | bytes 49152 | tf_op jit(solution)/shard_map/psum | solution.py:46
  41.2 0.1 reshape.76
  41.3 2.7 %copy.18 = bf16[8,768,128]{1,2,0:T(8,128)(2,1)} copy(bf16[8,768,128]{2,1,0:T(8,128)(2,1)} %param.21) | data formatting | bytes 3145728 | tf_op args[8]
  43.9 1.8 %fusion.33 = (f32[8,2,8]{2,1,0:T(2,128)S(1)}, f32[8,2,8,768]{3,2,1,0:T(8,128)S(1)}) fusion(f32[8,16,768]{2,1,0:T(8,128)S(1)} %copy-done.1, f32[8,16]{1,0:T(8,128)S(1)} %fusion.22, bf16[8,2,8,64]{3,2,1,0:T(8,128)(2,1)S(1)} %reshape.76, bf16[8,768,2,64]{1,3,2,0:T(8,128)(2,1)} %bitcast.24, pred[8,768]{1,0:T(8,128)(4,1)S(1)} %broadcast_compare_fusion), kind=kOutput, calls=%fused_computation.44 | convolution fusion | flops 13074304 | bytes 2382848 | tf_op jit(solution)/shard_map/skgd,spkd->skgp/dot_general | solution.py:60
  45.7 8.5 %pmax.7 = f32[8,2,8]{2,1,0:T(2,128)S(1)} all-reduce(f32[8,2,8]{2,1,0:T(2,128)S(1)} %get-tuple-element.12), channel_id=1, replica_groups=mesh['grp'=2,'kv'=4,'tp'=4] {'kv'}, use_global_device_ids=true, to_apply=%region_3.0 | all-reduce | flops 128 | bytes 1024 | tf_op jit(solution)/shard_map/pmax | solution.py:80
  54.3 0.2 fusion.3
  54.5 2.6 %copy.19 = bf16[8,768,128]{1,2,0:T(8,128)(2,1)} copy(bf16[8,768,128]{2,1,0:T(8,128)(2,1)} %param.22) | data formatting | bytes 3145728 | tf_op args[9]
  57.1 2.0 %convolution_multiply_fusion.1 = f32[8,2,8,64]{3,2,1,0:T(8,128)S(1)} fusion(bf16[8,768,2,64]{1,3,2,0:T(8,128)(2,1)} %bitcast.25, f32[8,2,8,768]{3,2,1,0:T(8,128)S(1)} %get-tuple-element.13, f32[8,2,8]{2,1,0:T(2,128)S(1)} %get-tuple-element.12, pred[8,768]{1,0:T(8,128)(4,1)S(1)} %broadcast_compare_fusion, f32[8,2,8]{2,1,0:T(2,128)S(1)} %bitcast.30), kind=kOutput, calls=%fused_computation.3 | convolution fusion | flops 12886016 | bytes 2006016 | tf_op jit(solution)/shard_map/skgp,spkd->skgd/dot_general | solution.py:74
  59.1 18.7 %all-reduce = (f32[8,2,8,64]{3,2,1,0:T(8,128)S(1)}, bf16[8,128]{1,0:T(8,128)(2,1)S(1)}, f32[8,2,8]{2,1,0:T(2,128)S(1)}, bf16[8,128]{1,0:T(8,128)(2,1)S(1)}) all-reduce(f32[8,2,8,64]{3,2,1,0:T(8,128)S(1)} %convolution_multiply_fusion.1, f32[8,128]{1,0:T(8,128)S(1)} %fusion.15, ...), channel_id=1, replica_groups=mesh['grp'=2,'kv'=4,'tp'=4] {'kv'}, use_global_device_ids=true, to_apply=%region_4.5 | all-reduce | flops 10368 | bytes 78848 | tf_op jit(solution)/shard_map/psum | solution.py:82
  77.9 0.1 fusion.34
  78.1 0.1 reshape.81
  78.1 0.1 divide_convert_fusion
  78.3 0.1 convert_element_type.49
  78.4 2.2 %convolution_convert_fusion = bf16[8,1024]{1,0:T(8,128)(2,1)S(1)} fusion(bf16[8,1024]{1,0:T(8,128)(2,1)S(1)} %convert_element_type.49, bf16[1024,1024]{1,0:T(8,128)(2,1)} %param.20), kind=kOutput, calls=%fused_computation.4 | convolution fusion | flops 16785408 | bytes 2129920 | tf_op jit(solution)/shard_map/dot_general | solution.py:103
  80.6 10.7 %psum.47 = bf16[8,1024]{1,0:T(8,128)(2,1)} all-reduce(bf16[8,1024]{1,0:T(8,128)(2,1)S(1)} %convolution_convert_fusion), channel_id=1, replica_groups=mesh['grp'=2,'kv'=4,'tp'=4] {'tp'}, use_global_device_ids=true, to_apply=%region_9.10 | all-reduce | flops 8192 | bytes 32768 | tf_op jit(solution)/shard_map/psum | solution.py:107
  (13 shorter events, 0.2 us)
Async XLA Ops:
  0.6 21.0 %copy-start = (bf16[1024,1024]{1,0:T(8,128)(2,1)S(1)}, bf16[1024,1024]{1,0:T(8,128)(2,1)}, u32[]{:S(2)}) copy-start(bf16[1024,1024]{1,0:T(8,128)(2,1)} %param.15) | copy-start | bytes 6291460
  41.3 2.7 %copy-start.1 = (f32[8,16,768]{2,1,0:T(8,128)S(1)}, f32[8,16,768]{2,1,0:T(8,128)}, u32[]{:S(2)}) copy-start(f32[8,16,768]{2,1,0:T(8,128)} %param.23) | copy-start | bytes 1179652
  77.8 13.5 %copy-start.2 = (bf16[8,128]{1,0:T(8,128)(2,1)}, bf16[8,128]{1,0:T(8,128)(2,1)S(1)}, u32[]{:S(2)}) copy-start(bf16[8,128]{1,0:T(8,128)(2,1)S(1)} %get-tuple-element.4) | copy-start | bytes 6148
  77.8 13.5 %copy-start.3 = (bf16[8,128]{1,0:T(8,128)(2,1)}, bf16[8,128]{1,0:T(8,128)(2,1)S(1)}, u32[]{:S(2)}) copy-start(bf16[8,128]{1,0:T(8,128)(2,1)S(1)} %get-tuple-element.6) | copy-start | bytes 6148
where the time goes:
time: 91.8 us; the launch traced here: 91.3 us
  blocking collectives  72.2 us (79%)
  matrix products  9.82 us (11%)
  local copies, waits for them, and re-layouts  6.53 us (7%)
  other arithmetic  2.09 us (2%)
    psum x1, blocking collectives, per_device(): lax.psum((query_part, key_part, value_part), 'kv')  19.1 us
    psum x1, blocking collectives, per_device(): lax.psum((local_total * rescale, local_values * rescale[..., None]), 'kv')  18.7 us
    all_gather x1, blocking collectives, per_device(): whole = lax.all_gather(tokens, 'kv', axis=1, tiled=True)  15.1 us
    psum x1, blocking collectives, per_device(): mixed = lax.psum(partial_value.astype(jnp.bfloat16), 'tp')  10.7 us
    pmax x1, blocking collectives, per_device(): block_max = lax.pmax(local_max, 'kv')  8.5 us
    unnamed x10, local copies, waits for them, and re-layouts  5.29 us
    dot_general x1, matrix products, per_device(): lax.dot_general(attended, w_out, (((1,), (1,)), ((), ())), preferred_elem...  2.23 us
    dot_general x1, matrix products, per_device(): jnp.einsum('skgp,spkd->skgd', weights.astype(jnp.bfloat16), value_block,...  1.98 us

commit v1 on v0

--- a/solution.py
+++ b/solution.py
@@ -104,7 +104,7 @@
         attended, w_out, (((1,), (1,)), ((), ())), preferred_element_type=jnp.float32
     )
     partial_value = lax.optimization_barrier(partial_value.astype(jnp.bfloat16)).astype(jnp.float32)
-    mixed = lax.psum(partial_value.astype(jnp.bfloat16), "tp")
+    mixed = jnp.sum(lax.all_gather(partial_value.astype(jnp.bfloat16), "tp"), axis=0)
     return (mixed, key_new, value_new)
 
 

time: 91.8 us -> 87 us (0.948)
  blocking collectives: 72.2 us -> 66.7 us
    psum x1 -> x0, blocking collectives: 10.7 us -> none  [per_device(): mixed = lax.psum(partial_value.astype(jnp.bfloat16), 'tp')]
    all_gather x0 -> x1, blocking collectives: none -> 5.24 us  [per_device(): lax.all_gather(partial_value.astype(jnp.bfloat16), 'tp')]
where the time goes in v1:
time: 87 us; the launch traced here: 86.5 us
  blocking collectives  66.7 us (77%)
  matrix products  9.82 us (11%)
  local copies, waits for them, and re-layouts  6.53 us (8%)
  other arithmetic  2.7 us (3%)
    psum x1, blocking collectives, per_device(): lax.psum((query_part, key_part, value_part), 'kv')  19.1 us
    psum x1, blocking collectives, per_device(): lax.psum((local_total * rescale, local_values * rescale[..., None]), 'kv')  18.7 us
    all_gather x1, blocking collectives, per_device(): whole = lax.all_gather(tokens, 'kv', axis=1, tiled=True)  15.1 us
    pmax x1, blocking collectives, per_device(): block_max = lax.pmax(local_max, 'kv')  8.5 us
    unnamed x10, local copies, waits for them, and re-layouts  5.29 us
    all_gather x1, blocking collectives, per_device(): lax.all_gather(partial_value.astype(jnp.bfloat16), 'tp')  5.24 us
    dot_general x1, matrix products, per_device(): lax.dot_general(attended, w_out, (((1,), (1,)), ((), ())), preferred_elem...  2.23 us
    dot_general x1, matrix products, per_device(): jnp.einsum('skgp,spkd->skgd', weights.astype(jnp.bfloat16), value_block,...  1.98 us

profile of v1, /device:TPU:0, one launch (start us, length us, event | category | flops | bytes accessed | tf_op | source)
XLA Modules:
  0.0 86.5 jit_solution(10388174928833785122)
XLA Ops:
  0.7 0.9 %dynamic_slice.11 = f32[16]{0:T(128)S(1)} dynamic-slice(f32[64]{0:T(128)} %param.19, s32[]{:T(128)S(6)} %select_n.20), dynamic_slice_sizes={16} | dynamic-slice | bytes 132 | tf_op jit(solution)/shard_map/dynamic_slice | solution.py:51
  1.5 0.7 broadcast_compare_fusion
  2.3 15.1 %all_gather.9 = bf16[8,4096]{1,0:T(8,128)(2,1)S(1)} all-gather(bf16[8,1024]{1,0:T(8,128)(2,1)} %param.13), channel_id=1, replica_groups=mesh['grp'=2,'kv'=4,'tp'=4] {'kv'}, dimensions={1}, use_global_device_ids=true | all-gather | bytes 81920 | tf_op jit(solution)/shard_map/all_gather | solution.py:32
  17.4 0.1 fusion.9
  17.5 0.8 fusion.11
  18.4 1.1 %fusion.22 = f32[8,16]{1,0:T(8,128)S(1)} fusion(f32[8,16]{1,0:T(8,128)} %param.24, bf16[8,4096]{1,0:T(8,128)(2,1)S(1)} %fusion.11, bf16[4096,64]{0,1:T(8,128)(2,1)} %param.18, s32[]{:T(128)S(6)} %select_n.20, f32[16]{0:T(128)S(1)} %dynamic_slice.11), kind=kOutput, calls=%fused_computation.36 | convolution fusion | flops 1049856 | bytes 201284 | tf_op jit(solution)/shard_map/dot_general | solution.py:53
  19.4 1.1 %fusion.15 = f32[8,128]{1,0:T(8,128)S(1)} fusion(bf16[1024,128]{1,0:T(8,128)(2,1)} %param.16, bf16[8,4096]{1,0:T(8,128)(2,1)S(1)} %fusion.11, s32[]{:T(128)S(6)} %select_n.19), kind=kOutput, calls=%fused_computation.25 | convolution fusion | flops 2097152 | bytes 282628 | tf_op jit(solution)/shard_map/dot_general | solution.py:44
  20.6 1.1 %fusion.13 = f32[8,128]{1,0:T(8,128)S(1)} fusion(bf16[1024,128]{1,0:T(8,128)(2,1)} %param.17, bf16[8,4096]{1,0:T(8,128)(2,1)S(1)} %fusion.11, s32[]{:T(128)S(6)} %select_n.19), kind=kOutput, calls=%fused_computation.23 | convolution fusion | flops 2097152 | bytes 282628 | tf_op jit(solution)/shard_map/dot_general | solution.py:45
  21.7 0.4 fusion.17
  22.0 19.1 %psum.35 = bf16[8,1024]{1,0:T(8,128)(2,1)S(1)} all-reduce(f32[8,1024]{1,0:T(8,128)S(1)} %fusion.17), channel_id=1, replica_groups=mesh['grp'=2,'kv'=4,'tp'=4] {'kv'}, use_global_device_ids=true, to_apply=%region_1.0 | all-reduce | flops 8192 | bytes 49152 | tf_op jit(solution)/shard_map/psum | solution.py:46
  41.2 0.1 reshape.76
  41.3 2.7 %copy.18 = bf16[8,768,128]{1,2,0:T(8,128)(2,1)} copy(bf16[8,768,128]{2,1,0:T(8,128)(2,1)} %param.21) | data formatting | bytes 3145728 | tf_op args[8]
  43.9 1.8 %fusion.33 = (f32[8,2,8]{2,1,0:T(2,128)S(1)}, f32[8,2,8,768]{3,2,1,0:T(8,128)S(1)}) fusion(f32[8,16,768]{2,1,0:T(8,128)S(1)} %copy-done.1, f32[8,16]{1,0:T(8,128)S(1)} %fusion.22, bf16[8,2,8,64]{3,2,1,0:T(8,128)(2,1)S(1)} %reshape.76, bf16[8,768,2,64]{1,3,2,0:T(8,128)(2,1)} %bitcast.26, pred[8,768]{1,0:T(8,128)(4,1)S(1)} %broadcast_compare_fusion), kind=kOutput, calls=%fused_computation.45 | convolution fusion | flops 13074304 | bytes 2382848 | tf_op jit(solution)/shard_map/skgd,spkd->skgp/dot_general | solution.py:60
  45.7 8.5 %pmax.7 = f32[8,2,8]{2,1,0:T(2,128)S(1)} all-reduce(f32[8,2,8]{2,1,0:T(2,128)S(1)} %get-tuple-element.12), channel_id=1, replica_groups=mesh['grp'=2,'kv'=4,'tp'=4] {'kv'}, use_global_device_ids=true, to_apply=%region_3.0 | all-reduce | flops 128 | bytes 1024 | tf_op jit(solution)/shard_map/pmax | solution.py:80
  54.3 0.2 fusion.3
  54.5 2.6 %copy.19 = bf16[8,768,128]{1,2,0:T(8,128)(2,1)} copy(bf16[8,768,128]{2,1,0:T(8,128)(2,1)} %param.22) | data formatting | bytes 3145728 | tf_op args[9]
  57.1 2.0 %convolution_multiply_fusion.1 = f32[8,2,8,64]{3,2,1,0:T(8,128)S(1)} fusion(bf16[8,768,2,64]{1,3,2,0:T(8,128)(2,1)} %bitcast.27, f32[8,2,8,768]{3,2,1,0:T(8,128)S(1)} %get-tuple-element.13, f32[8,2,8]{2,1,0:T(2,128)S(1)} %get-tuple-element.12, pred[8,768]{1,0:T(8,128)(4,1)S(1)} %broadcast_compare_fusion, f32[8,2,8]{2,1,0:T(2,128)S(1)} %bitcast.32), kind=kOutput, calls=%fused_computation.3 | convolution fusion | flops 12886016 | bytes 2006016 | tf_op jit(solution)/shard_map/skgp,spkd->skgd/dot_general | solution.py:74
  59.1 18.7 %all-reduce = (f32[8,2,8,64]{3,2,1,0:T(8,128)S(1)}, bf16[8,128]{1,0:T(8,128)(2,1)S(1)}, f32[8,2,8]{2,1,0:T(2,128)S(1)}, bf16[8,128]{1,0:T(8,128)(2,1)S(1)}) all-reduce(f32[8,2,8,64]{3,2,1,0:T(8,128)S(1)} %convolution_multiply_fusion.1, f32[8,128]{1,0:T(8,128)S(1)} %fusion.15, ...), channel_id=1, replica_groups=mesh['grp'=2,'kv'=4,'tp'=4] {'kv'}, use_global_device_ids=true, to_apply=%region_4.5 | all-reduce | flops 10368 | bytes 78848 | tf_op jit(solution)/shard_map/psum | solution.py:82
  77.9 0.1 fusion.34
  78.1 0.1 divide_convert_fusion
  78.3 0.1 convert_element_type.51
  78.4 2.2 %convolution_convert_fusion = bf16[8,1024]{1,0:T(8,128)(2,1)S(1)} fusion(bf16[8,1024]{1,0:T(8,128)(2,1)S(1)} %convert_element_type.51, bf16[1024,1024]{1,0:T(8,128)(2,1)} %param.20), kind=kOutput, calls=%fused_computation.4 | convolution fusion | flops 16785408 | bytes 2129920 | tf_op jit(solution)/shard_map/dot_general | solution.py:103
  80.6 5.2 %all-gather = bf16[32,1024]{1,0:T(8,128)(2,1)S(1)} all-gather(bf16[8,1024]{1,0:T(8,128)(2,1)S(1)} %convolution_convert_fusion), channel_id=2, replica_groups=mesh['grp'=2,'kv'=4,'tp'=4] {'tp'}, dimensions={0}, use_global_device_ids=true | all-gather | bytes 81920 | tf_op jit(solution)/shard_map/all_gather | solution.py:107
  85.8 0.6 bitcast_reduce_fusion
  (14 shorter events, 0.2 us)
Async XLA Ops:
  0.6 21.0 %copy-start = (bf16[1024,1024]{1,0:T(8,128)(2,1)S(1)}, bf16[1024,1024]{1,0:T(8,128)(2,1)}, u32[]{:S(2)}) copy-start(bf16[1024,1024]{1,0:T(8,128)(2,1)} %param.15) | copy-start | bytes 6291460
  41.3 2.7 %copy-start.1 = (f32[8,16,768]{2,1,0:T(8,128)S(1)}, f32[8,16,768]{2,1,0:T(8,128)}, u32[]{:S(2)}) copy-start(f32[8,16,768]{2,1,0:T(8,128)} %param.23) | copy-start | bytes 1179652
  77.8 8.7 %copy-start.2 = (bf16[8,128]{1,0:T(8,128)(2,1)}, bf16[8,128]{1,0:T(8,128)(2,1)S(1)}, u32[]{:S(2)}) copy-start(bf16[8,128]{1,0:T(8,128)(2,1)S(1)} %get-tuple-element.4) | copy-start | bytes 6148
  77.8 8.7 %copy-start.3 = (bf16[8,128]{1,0:T(8,128)(2,1)}, bf16[8,128]{1,0:T(8,128)(2,1)S(1)}, u32[]{:S(2)}) copy-start(bf16[8,128]{1,0:T(8,128)(2,1)S(1)} %get-tuple-element.6) | copy-start | bytes 6148
